TPU v7x, 32 devices: a whole 2x2x4 slice. The times are simulated.
32 devices in a mesh: rep: 2 (over x), fs: 8 (over z, y), tp: 2 (over core).
Axes of the slice: x: 2, y: 2, z: 4, core: 2. Of those that a mesh axis runs over, the one named last changes fastest.
Arguments:
- hidden_in: bfloat16 [12288, 2048], P(('rep', 'fs', 'tp')), may hold values from -6 to 6
- norm_gain: float32 [2048], replicated, may hold values from 0.1 to 1.9
- up_weight: float32 [2048, 8192], P('fs', 'tp'), may hold values from -0.125 to 0.125
- up_scale: float32 [8192], P('tp'), may hold values from 0.5 to 2
- down_weight: float32 [8192, 2048], P('tp', 'fs'), may hold values from -0.0625 to 0.0625
- down_scale: float32 [2048], replicated, may hold values from 0.5 to 2
Outputs:
- layer_out: bfloat16 [12288, 2048], P(('rep', 'fs', 'tp'))
All inputs are finite; a program needn't handle non-finite values.
Results may differ from a plain program's by a relative error of at most 0.0085.
Values may be sent and summed in bfloat16 or wider, within the bound.
A program may use at most 128 MiB of HBM per device.

v0:
```python
import jax
import jax.numpy as jnp
from jax import lax
from jax.sharding import PartitionSpec as P


def body(hidden_in, norm_gain, up_weight, up_scale, down_weight, down_scale):
    rows = hidden_in.astype(jnp.float32)
    normed = (
        rows * lax.rsqrt(jnp.mean(rows * rows, axis=1, keepdims=True) + 1e-06) * norm_gain
    ).astype(jnp.bfloat16)
    gathered = lax.all_gather(normed, "tp", axis=0, tiled=True)
    up_low = up_weight.astype(jnp.bfloat16)
    down_low = down_weight.astype(jnp.bfloat16)
    up_whole = lax.all_gather(up_low, "fs", axis=0, tiled=True)
    pre = jnp.dot(gathered, up_whole, preferred_element_type=jnp.float32)
    down_whole = lax.all_gather(down_low, "fs", axis=1, tiled=True)
    act = jnp.square(jnp.maximum(pre * up_scale, 0.0)).astype(jnp.bfloat16)
    summed = lax.psum_scatter(
        jnp.dot(act, down_whole, preferred_element_type=jnp.float32).astype(jnp.bfloat16),
        "tp",
        scatter_dimension=0,
        tiled=True,
    ).astype(jnp.float32)
    return (summed * down_scale).astype(jnp.bfloat16)


def solution(mesh):
    placed = (P(("rep", "fs", "tp"), None), P(), P("fs", "tp"), P("tp"), P("tp", "fs"), P())
    return jax.shard_map(
        body, mesh=mesh, in_specs=placed, out_specs=P(("rep", "fs", "tp"), None), check_vma=False
    )
```

profile of v0, /device:TPU:0, one launch (start us, length us, event | category | flops | bytes accessed | tf_op | source)
XLA Modules:
  0.0 542.0 jit_solution(9499222584294802348)
XLA Ops:
  6.5 0.0 all-gather.4.cloned.1.call-start
  6.5 1.8 fusion
  8.3 3.0 fusion.2
  11.3 0.0 all-gather.4.cloned.1.call-update
  11.3 0.0 all-gather.6.cloned.1.call-start
  11.4 3.8 convert_element_type.26
  15.2 0.0 all-gather.6.cloned.1.call-update
  15.3 0.0 copy-start.1
  15.3 0.0 all-gather.8.cloned.1.call-start
  15.3 3.7 convert_element_type.28
  19.0 0.0 all-gather.8.cloned.1.call-update
  19.1 0.0 reduce-scatter.2.cloned.1.call-start
  19.1 7.2 %all-gather.4.cloned.1.call-done = bf16[768,2048]{1,0:T(8,128)(2,1)} async-done(((bf16[384,2048]{1,0:T(8,128)(2,1)}), bf16[768,2048]{1,0:T(8,128)(2,1)}) %all-gather.4.cloned.1.call-update) | async-done | bytes 3145744 | tf_op jit(solution)/shard_map/all_gather | solution.py:12
  26.3 230.6 %all-gather.6.cloned.1.call-done = bf16[2048,4096]{1,0:T(8,128)(2,1)} async-done(((bf16[256,4096]{1,0:T(8,128)(2,1)}), bf16[2048,4096]{1,0:T(8,128)(2,1)}) %all-gather.6.cloned.1.call-update) | async-done | bytes 16777232 | tf_op jit(solution)/shard_map/all_gather | solution.py:15
  257.0 227.6 %all-gather.8.cloned.1.call-done = bf16[4096,2048]{1,0:T(8,128)(2,1)} async-done(((bf16[4096,256]{1,0:T(8,128)(2,1)}), bf16[4096,2048]{1,0:T(8,128)(2,1)}) %all-gather.8.cloned.1.call-update) | async-done | bytes 16777232 | tf_op jit(solution)/shard_map/all_gather | solution.py:17
  484.5 0.0 copy-done.1
  484.5 38.5 %convolution_convert_fusion = bf16[768,2048]{1,0:T(8,128)(2,1)} fusion(bf16[4096,2048]{1,0:T(8,128)(2,1)} %all-gather.8.cloned.1.call-done, bf16[768,2048]{1,0:T(8,128)(2,1)} %all-gather.4.cloned.1.call-done, bf16[2048,4096]{1,0:T(8,128)(2,1)} %all-gather.6.cloned.1.call-done, f32[4096]{0:T(1024)S(1)} %copy-done.1), kind=kOutput, calls=%fused_computation.3 | convolution fusion | flops 25783959552 | bytes 39862272 | tf_op jit(solution)/shard_map/dot_general | solution.py:20
  523.0 0.0 copy-start
  523.0 0.0 reduce-scatter.2.cloned.1.call-update
  523.0 9.5 %reduce-scatter.2.cloned.1.call-done = bf16[384,2048]{1,0:T(8,128)(2,1)} async-done(((bf16[768,2048]{1,0:T(8,128)(2,1)}), bf16[384,2048]{1,0:T(8,128)(2,1)}) %reduce-scatter.2.cloned.1.call-update) | async-done | bytes 1572880 | tf_op jit(solution)/shard_map/reduce_scatter | solution.py:19
  532.6 0.0 copy-done
  532.6 2.9 multiply_convert_fusion.1
  (1 shorter events, 0.0 us)
Async XLA Ops:
  6.5 19.8 %all-gather.4.cloned.1.call-start = ((), (), s32[]{:S(2)}) async-start(), calls=%async_computation.1 | async-start | bytes 4718592 | tf_op jit(solution)/shard_map/all_gather | solution.py:12
  11.3 245.6 %all-gather.6.cloned.1.call-start = ((), (), s32[]{:S(2)}) async-start(), calls=%async_computation.2 | async-start | bytes 18874368 | tf_op jit(solution)/shard_map/all_gather | solution.py:15
  15.3 469.3 %copy-start.1 = (f32[4096]{0:T(1024)S(1)}, f32[4096]{0:T(1024)}, u32[]{:S(2)}) copy-start(f32[4096]{0:T(1024)} %param.9) | copy-start | bytes 49156
  15.3 469.3 %all-gather.8.cloned.1.call-start = ((), (), s32[]{:S(2)}) async-start(), calls=%async_computation.3 | async-start | bytes 18874368 | tf_op jit(solution)/shard_map/all_gather | solution.py:17
  19.1 513.5 %reduce-scatter.2.cloned.1.call-start = ((), (), s32[]{:S(2)}) async-start(), calls=%async_computation.4 | async-start | bytes 4718592 | tf_op jit(solution)/shard_map/reduce_scatter | solution.py:19
  523.0 9.5 %copy-start = (f32[2048]{0:T(1024)S(1)}, f32[2048]{0:T(1024)}, u32[]{:S(2)}) copy-start(f32[2048]{0:T(1024)} %param.11) | copy-start | bytes 24580
Sparse Core Ops, SparseCore 0:
  11.5 14.8 all-gather.3
  28.5 228.4 all-gather.5
  259.0 225.4 all-gather.7
  523.2 9.3 reduce-scatter.1
where the time goes:
time: 542 us
  waiting for transfers between devices  475 us (88%)
  matrix products  38.5 us (7%)
  other arithmetic  15.3 us (3%)
  between operations  13.1 us (2%)
    all_gather x1, waiting for transfers between devices, body(): up_whole = lax.all_gather(up_low, 'fs', axis=0, tiled=True)  231 us
    all_gather x1, waiting for transfers between devices, body(): down_whole = lax.all_gather(down_low, 'fs', axis=1, tiled=True)  228 us
    dot_general x1, matrix products, body(): jnp.dot(act, down_whole, preferred_element_type=jnp.float32)  38.5 us
  transfers between devices with their start and end apart: 4, of which 4 were waited for; matrix products, arithmetic and copies ran while one was open for 1% of the time, Pallas kernels for 0%

commit v1 on v0

--- a/solution.py
+++ b/solution.py
@@ -12,7 +12,12 @@
     gathered = lax.all_gather(normed, "tp", axis=0, tiled=True)
     up_low = up_weight.astype(jnp.bfloat16)
     down_low = down_weight.astype(jnp.bfloat16)
-    up_whole = lax.all_gather(up_low, "fs", axis=0, tiled=True)
+    ring = [up_low]
+    for hop in range(7):
+        ring.append(lax.ppermute(ring[-1], "fs", [(dev, (dev + 1) % 8) for dev in range(8)]))
+    up_whole = jnp.roll(
+        jnp.concatenate(ring[::-1], axis=0), (lax.axis_index("fs") + 1) * ring[0].shape[0], axis=0
+    )
     pre = jnp.dot(gathered, up_whole, preferred_element_type=jnp.float32)
     down_whole = lax.all_gather(down_low, "fs", axis=1, tiled=True)
     act = jnp.square(jnp.maximum(pre * up_scale, 0.0)).astype(jnp.bfloat16)

time: 542 us -> 643 us (1.19)
  waiting for transfers between devices: 475 us -> 536 us
  local copies, waits for them, and re-layouts: 0.01 us -> 34.6 us
    ppermute x0 -> x7, waiting for transfers between devices: none -> 528 us  [body(): lax.ppermute(ring[-1], 'fs', [(dev, (dev + 1) % 8) for dev in range(8)])]
    all_gather x1 -> x0, waiting for transfers between devices: 231 us -> none  [body(): up_whole = lax.all_gather(up_low, 'fs', axis=0, tiled=True)]
    all_gather x1, waiting for transfers between devices: 228 us -> 0.01 us  [body(): down_whole = lax.all_gather(down_low, 'fs', axis=1, tiled=True)]
    unnamed x4 -> x36, local copies, waits for them, and re-layouts: 0.01 us -> 34.6 us
    dot_general x0 -> x1, matrix products: none -> 19.2 us  [body(): pre = jnp.dot(gathered, up_whole, preferred_element_type=jnp.float32)]
    dot_general x1, matrix products: 38.5 us -> 19.7 us  [body(): jnp.dot(act, down_whole, preferred_element_type=jnp.float32)]
    all_gather x1, waiting for transfers between devices: 7.24 us -> 0.01 us  [body(): gathered = lax.all_gather(normed, 'tp', axis=0, tiled=True)]
  transfers between devices with their start and end apart: 4 -> 10, of which waited for: 4 -> 8; matrix products, arithmetic and copies ran while one was open for 1% -> 9% of each run, Pallas kernels for 0% -> 0%
where the time goes in v1:
time: 643 us
  waiting for transfers between devices  536 us (83%)
  matrix products  38.9 us (6%)
  local copies, waits for them, and re-layouts  34.6 us (5%)
  other arithmetic  17.1 us (3%)
  between operations  13.1 us (2%)
    ppermute x7, waiting for transfers between devices, body(): lax.ppermute(ring[-1], 'fs', [(dev, (dev + 1) % 8) for dev in range(8)])  528 us
    unnamed x36, local copies, waits for them, and re-layouts  34.6 us
    dot_general x1, matrix products, body(): jnp.dot(act, down_whole, preferred_element_type=jnp.float32)  19.7 us
    dot_general x1, matrix products, body(): pre = jnp.dot(gathered, up_whole, preferred_element_type=jnp.float32)  19.2 us
  transfers between devices with their start and end apart: 10, of which 8 were waited for; matrix products, arithmetic and copies ran while one was open for 9% of the time, Pallas kernels for 0%

profile of v1, /device:TPU:0, one launch (start us, length us, event | category | flops | bytes accessed | tf_op | source)
XLA Modules:
  0.0 643.0 jit_solution(11948466008937606953)
XLA Ops:
  6.5 1.8 fusion.4
  8.3 3.0 fusion.6
  11.4 3.7 convert_element_type.28
  15.2 2.5 convert_element_type.26
  17.6 3.0 collective-permute-start
  20.7 72.1 %collective-permute-done = bf16[256,4096]{1,0:T(8,128)(2,1)S(1)} collective-permute-done((bf16[256,4096]{1,0:T(8,128)(2,1)S(1)}, bf16[256,4096]{1,0:T(8,128)(2,1)S(1)}, u32[]{:S(2)}, u32[]{:S(2)}) %collective-permute-start) | collective-permute-done | bytes 2097184 | tf_op jit(solution)/shard_map/ppermute | solution.py:17
  92.8 89.0 %collective-permute-done.1 = bf16[256,4096]{1,0:T(8,128)(2,1)S(1)} collective-permute-done((bf16[256,4096]{1,0:T(8,128)(2,1)S(1)}, bf16[256,4096]{1,0:T(8,128)(2,1)S(1)}, u32[]{:S(2)}, u32[]{:S(2)}) %collective-permute-start.1) | collective-permute-done | bytes 2097184 | tf_op jit(solution)/shard_map/ppermute | solution.py:17
  183.2 95.6 %collective-permute-done.2 = bf16[256,4096]{1,0:T(8,128)(2,1)S(1)} collective-permute-done((bf16[256,4096]{1,0:T(8,128)(2,1)S(1)}, bf16[256,4096]{1,0:T(8,128)(2,1)S(1)}, u32[]{:S(2)}, u32[]{:S(2)}) %collective-permute-start.2) | collective-permute-done | bytes 2097184 | tf_op jit(solution)/shard_map/ppermute | solution.py:17
  280.2 95.4 %collective-permute-done.3 = bf16[256,4096]{1,0:T(8,128)(2,1)S(1)} collective-permute-done((bf16[256,4096]{1,0:T(8,128)(2,1)S(1)}, bf16[256,4096]{1,0:T(8,128)(2,1)S(1)}, u32[]{:S(2)}, u32[]{:S(2)}) %collective-permute-start.3) | collective-permute-done | bytes 2097184 | tf_op jit(solution)/shard_map/ppermute | solution.py:17
  376.8 77.3 %collective-permute-done.4 = bf16[256,4096]{1,0:T(8,128)(2,1)S(1)} collective-permute-done((bf16[256,4096]{1,0:T(8,128)(2,1)S(1)}, bf16[256,4096]{1,0:T(8,128)(2,1)S(1)}, u32[]{:S(2)}, u32[]{:S(2)}) %collective-permute-start.4) | collective-permute-done | bytes 2097184 | tf_op jit(solution)/shard_map/ppermute | solution.py:17
  455.4 49.4 %collective-permute-done.5 = bf16[256,4096]{1,0:T(8,128)(2,1)} collective-permute-done((bf16[256,4096]{1,0:T(8,128)(2,1)S(1)}, bf16[256,4096]{1,0:T(8,128)(2,1)}, u32[]{:S(2)}, u32[]{:S(2)}) %collective-permute-start.5) | collective-permute-done | bytes 2097184 | tf_op jit(solution)/shard_map/ppermute | solution.py:17
  504.9 48.8 %collective-permute-done.6 = bf16[256,4096]{1,0:T(8,128)(2,1)} collective-permute-done((bf16[256,4096]{1,0:T(8,128)(2,1)}, bf16[256,4096]{1,0:T(8,128)(2,1)}, u32[]{:S(2)}, u32[]{:S(2)}) %collective-permute-start.6) | collective-permute-done | bytes 2097184 | tf_op jit(solution)/shard_map/ppermute | solution.py:17
  553.7 3.1 constant_dynamic-update-slice_fusion.15
  556.8 3.3 constant_dynamic-update-slice_fusion.14
  560.1 3.2 constant_dynamic-update-slice_fusion.13
  563.2 1.5 constant_dynamic-update-slice_fusion.12
  564.7 1.5 constant_dynamic-update-slice_fusion.11
  566.3 1.5 constant_dynamic-update-slice_fusion.10
  567.7 1.5 constant_dynamic-update-slice_fusion.9
  569.2 1.6 constant_dynamic-update-slice_fusion.8
  570.8 3.1 constant_dynamic-update-slice_fusion.7
  574.0 3.1 constant_dynamic-update-slice_fusion.6
  577.1 1.5 constant_dynamic-update-slice_fusion.5
  578.6 1.5 constant_dynamic-update-slice_fusion.4
  580.1 1.5 constant_dynamic-update-slice_fusion.3
  581.6 1.5 constant_dynamic-update-slice_fusion.2
  583.1 1.5 constant_dynamic-update-slice_fusion.1
  584.5 1.6 constant_dynamic-update-slice_fusion
  586.1 19.2 %multiply_convert_fusion.clone.4 = bf16[768,4096]{1,0:T(8,128)(2,1)} fusion(bf16[768,2048]{1,0:T(8,128)(2,1)} %all-gather.3.cloned.1.call-done, bf16[4096,4096]{1,0:T(8,128)(2,1)} %constant_dynamic-update-slice_fusion, s32[]{:T(128)S(6)} %select_n.14, f32[4096]{0:T(1024)S(1)} %copy-done.10), kind=kOutput, calls=%fused_computation.2.clone.clone.clone.1 | convolution fusion | flops 12897484800 | bytes 26230788 | tf_op jit(solution)/shard_map/dot_general | solution.py:21
  605.4 19.7 %convolution_convert_fusion = bf16[768,2048]{1,0:T(8,128)(2,1)} fusion(bf16[4096,2048]{1,0:T(8,128)(2,1)} %all-gather.5.cloned.1.call-done, bf16[768,4096]{1,0:T(8,128)(2,1)} %multiply_convert_fusion.clone.4), kind=kOutput, calls=%fused_computation.5 | convolution fusion | flops 12886474752 | bytes 26214400 | tf_op jit(solution)/shard_map/dot_general | solution.py:25
  625.1 8.5 %reduce-scatter.2.cloned.1.call-done = bf16[384,2048]{1,0:T(8,128)(2,1)} async-done(((bf16[768,2048]{1,0:T(8,128)(2,1)}), bf16[384,2048]{1,0:T(8,128)(2,1)}) %reduce-scatter.2.cloned.1.call-update) | async-done | bytes 1572880 | tf_op jit(solution)/shard_map/reduce_scatter | solution.py:24
  633.6 2.9 multiply_convert_fusion.1
  (37 shorter events, 5.5 us)
Async XLA Ops:
  6.5 579.6 %all-gather.3.cloned.1.call-start = ((), (), s32[]{:S(2)}) async-start(), calls=%async_computation.1 | async-start | bytes 4718592 | tf_op jit(solution)/shard_map/all_gather | solution.py:12
  11.3 594.0 %all-gather.5.cloned.1.call-start = ((), (), s32[]{:S(2)}) async-start(), calls=%async_computation.2 | async-start | bytes 18874368 | tf_op jit(solution)/shard_map/all_gather | solution.py:22
  15.1 618.5 %reduce-scatter.2.cloned.1.call-start = ((), (), s32[]{:S(2)}) async-start(), calls=%async_computation.3 | async-start | bytes 4718592 | tf_op jit(solution)/shard_map/reduce_scatter | solution.py:24
  17.6 75.1 %collective-permute-start = (bf16[256,4096]{1,0:T(8,128)(2,1)S(1)}, bf16[256,4096]{1,0:T(8,128)(2,1)S(1)}, u32[]{:S(2)}, u32[]{:S(2)}) collective-permute-start(bf16[256,4096]{1,0:T(8,128)(2,1)S(1)} %convert_element_type.26), channel_id=1, source_target_pairs={{0,2},{2,4},{4,6},{6,8},{8,10},{10,12},{12,14},{14,0},{1,3},{3,5},... | collective-permute-start | bytes 6291464 | tf_op jit(solution)/shard_map/ppermute | solution.py:17
  92.8 89.0 %collective-permute-start.1 = (bf16[256,4096]{1,0:T(8,128)(2,1)S(1)}, bf16[256,4096]{1,0:T(8,128)(2,1)S(1)}, u32[]{:S(2)}, u32[]{:S(2)}) collective-permute-start(bf16[256,4096]{1,0:T(8,128)(2,1)S(1)} %collective-permute-done), channel_id=1, source_target_pairs={{0,2},{2,4},{4,6},{6,8},{8,10},{10,12},{12,14},{14,0},{1,3},{3,5},... | collective-permute-start | bytes 6291464 | tf_op jit(solution)/shard_map/ppermute | solution.py:17
  181.8 1.4 copy-start.1
  183.2 95.6 %collective-permute-start.2 = (bf16[256,4096]{1,0:T(8,128)(2,1)S(1)}, bf16[256,4096]{1,0:T(8,128)(2,1)S(1)}, u32[]{:S(2)}, u32[]{:S(2)}) collective-permute-start(bf16[256,4096]{1,0:T(8,128)(2,1)S(1)} %collective-permute-done.1), channel_id=1, source_target_pairs={{0,2},{2,4},{4,6},{6,8},{8,10},{10,12},{12,14},{14,0},{1,3},{3,5},... | collective-permute-start | bytes 6291464 | tf_op jit(solution)/shard_map/ppermute | solution.py:17
  278.8 1.3 copy-start.3
  280.2 95.4 %collective-permute-start.3 = (bf16[256,4096]{1,0:T(8,128)(2,1)S(1)}, bf16[256,4096]{1,0:T(8,128)(2,1)S(1)}, u32[]{:S(2)}, u32[]{:S(2)}) collective-permute-start(bf16[256,4096]{1,0:T(8,128)(2,1)S(1)} %collective-permute-done.2), channel_id=1, source_target_pairs={{0,2},{2,4},{4,6},{6,8},{8,10},{10,12},{12,14},{14,0},{1,3},{3,5},... | collective-permute-start | bytes 6291464 | tf_op jit(solution)/shard_map/ppermute | solution.py:17
  375.5 1.3 copy-start.5
  376.8 77.3 %collective-permute-start.4 = (bf16[256,4096]{1,0:T(8,128)(2,1)S(1)}, bf16[256,4096]{1,0:T(8,128)(2,1)S(1)}, u32[]{:S(2)}, u32[]{:S(2)}) collective-permute-start(bf16[256,4096]{1,0:T(8,128)(2,1)S(1)} %collective-permute-done.3), channel_id=1, source_target_pairs={{0,2},{2,4},{4,6},{6,8},{8,10},{10,12},{12,14},{14,0},{1,3},{3,5},... | collective-permute-start | bytes 6291464 | tf_op jit(solution)/shard_map/ppermute | solution.py:17
  454.1 1.3 copy-start.7
  455.4 49.4 %collective-permute-start.5 = (bf16[256,4096]{1,0:T(8,128)(2,1)S(1)}, bf16[256,4096]{1,0:T(8,128)(2,1)}, u32[]{:S(2)}, u32[]{:S(2)}) collective-permute-start(bf16[256,4096]{1,0:T(8,128)(2,1)S(1)} %collective-permute-done.4), channel_id=1, source_target_pairs={{0,2},{2,4},{4,6},{6,8},{8,10},{10,12},{12,14},{14,0},{1,3},{3,5},... | collective-permute-start | bytes 6291464 | tf_op jit(solution)/shard_map/ppermute | solution.py:17
  504.9 48.8 %collective-permute-start.6 = (bf16[256,4096]{1,0:T(8,128)(2,1)}, bf16[256,4096]{1,0:T(8,128)(2,1)}, u32[]{:S(2)}, u32[]{:S(2)}) collective-permute-start(bf16[256,4096]{1,0:T(8,128)(2,1)} %collective-permute-done.5), channel_id=1, source_target_pairs={{0,2},{2,4},{4,6},{6,8},{8,10},{10,12},{12,14},{14,0},{1,3},{3,5},... | collective-permute-start | bytes 6291464 | tf_op jit(solution)/shard_map/ppermute | solution.py:17
  504.9 58.4 %copy-start.6 = (bf16[256,4096]{1,0:T(8,128)(2,1)S(1)}, bf16[256,4096]{1,0:T(8,128)(2,1)}, u32[]{:S(2)}) copy-start(bf16[256,4096]{1,0:T(8,128)(2,1)} %copy-done.5) | copy-start | bytes 6291460
  504.9 59.9 %copy-start.4 = (bf16[256,4096]{1,0:T(8,128)(2,1)S(1)}, bf16[256,4096]{1,0:T(8,128)(2,1)}, u32[]{:S(2)}) copy-start(bf16[256,4096]{1,0:T(8,128)(2,1)} %copy-done.3) | copy-start | bytes 6291460
  504.9 61.4 %copy-start.2 = (bf16[256,4096]{1,0:T(8,128)(2,1)S(1)}, bf16[256,4096]{1,0:T(8,128)(2,1)}, u32[]{:S(2)}) copy-start(bf16[256,4096]{1,0:T(8,128)(2,1)} %copy-done.1) | copy-start | bytes 6291460
  556.8 12.4 %copy-start = (f32[256,4096]{1,0:T(8,128)S(1)}, f32[256,4096]{1,0:T(8,128)}, u32[]{:S(2)}) copy-start(f32[256,4096]{1,0:T(8,128)} %param.8) | copy-start | bytes 12582916
  566.3 10.8 %copy-start.8 = (bf16[256,4096]{1,0:T(8,128)(2,1)S(1)}, bf16[256,4096]{1,0:T(8,128)(2,1)}, u32[]{:S(2)}) copy-start(bf16[256,4096]{1,0:T(8,128)(2,1)} %copy-done.7) | copy-start | bytes 6291460
  578.6 7.6 %copy-start.10 = (f32[4096]{0:T(1024)S(1)}, f32[4096]{0:T(1024)}, u32[]{:S(2)}) copy-start(f32[4096]{0:T(1024)} %param.9) | copy-start | bytes 49156
  605.4 28.2 %copy-start.9 = (f32[2048]{0:T(1024)S(1)}, f32[2048]{0:T(1024)}, u32[]{:S(2)}) copy-start(f32[2048]{0:T(1024)} %param.11) | copy-start | bytes 24580
Sparse Core Ops, SparseCore 0:
  11.5 14.8 all-gather.2
  28.4 371.5 all-gather.4
  625.2 8.3 reduce-scatter.1
